TPU v7x, 32 devices: a whole 2x2x4 slice. The times are simulated.
32 devices in a mesh: grp: 2 (over x), sp: 4 (over y, core), tp: 4 (over z).
Axes of the slice: x: 2, y: 2, z: 4, core: 2. Of those that a mesh axis runs over, the one named last changes fastest.
Arguments:
- residual: bfloat16 [768, 8, 2048], P(('sp', 'tp'), 'grp'), parts along dimension 1, may hold values from -6 to 6
- query: bfloat16 [768, 8, 1536], P('sp', 'grp', 'tp'), parts along dimension 1, may hold values from -64 to 64
- latent: bfloat16 [768, 8, 512], P('sp', 'grp'), parts along dimension 1, may hold values from -6 to 6
- rope_key: bfloat16 [768, 8, 64], P('sp', 'grp'), parts along dimension 1, may hold values from -8 to 8
- latent_gain: float32 [512], replicated, may hold values from 0.1 to 1.9
- key_up: bfloat16 [512, 1024], P(None, 'tp'), may hold values from -0.25 to 0.25
- value_up: bfloat16 [512, 1024], P(None, 'tp'), may hold values from -0.25 to 0.25
- out_weight: bfloat16 [1024, 2048], P('tp'), may hold values from -0.375 to 0.375
- norm_gain: float32 [2048], replicated, may hold values from 0.1 to 1.9
- group_prob: float32 [768, 8], P(('sp', 'tp'), 'grp'), parts along dimension 1, may hold values from 0.25 to 1
- pair_logits: float32 [768, 8, 2], P(('sp', 'tp'), 'grp'), parts along dimension 1, may hold values from -8 to 8
- routes: int32 [768, 8, 2], P(('sp', 'tp'), 'grp'), parts along dimension 1, may hold values from 0 to 15, all different within a row; in each aligned block of 192 rows (0 to 191, 192 to 383, ..., all dimensions but the last counted through in order) at most 36 rows name the same one
- w_gate: bfloat16 [16, 2048, 768], P(('sp', 'tp')), may hold values from -0.125 to 0.125
- w_up: bfloat16 [16, 2048, 768], P(('sp', 'tp')), may hold values from -0.125 to 0.125
- w_down: bfloat16 [16, 768, 2048], P(('sp', 'tp')), may hold values from -0.4375 to 0.4375
Outputs:
- layer_out: bfloat16 [768, 8, 2048], P(('sp', 'tp'), 'grp'), parts along dimension 1
There are 2 independent parts, one for each index of `grp`. A program takes and returns all parts, laid end to end along the dimension named above; an argument that names none is the same for every part. Nothing has to cross between parts.
Inputs may be any that keep to these rules, and one draw needn't show every extreme that they name: `routes`: A token's 2 experts differ. Among the tokens of one device (aligned blocks of 192 rows in position-then-sequence order), no expert is named more than 36 times, a bound that some block reaches.
All inputs are finite; a program needn't handle non-finite values.
Results may differ from a plain program's by a relative error of at most 0.013.
Values may be sent and summed in bfloat16 or wider, within the bound.
A program may use at most 128 MiB of HBM per device.

v0:
```python
import jax
import jax.numpy as jnp
from jax import lax
from jax.sharding import PartitionSpec as P

D = 2048
NOPE = 128
VDIM = 128
QK = 192
TOPK = 2
SEQS = 4
epsilon = 1e-06
rotary_base = 10000.0
lowest = -1e30


def rotate(values, positions):
    halfway = values.shape[-1] // 2
    inverse = rotary_base ** (-jnp.arange(halfway, dtype=jnp.float32) / halfway)
    angles = positions.astype(jnp.float32)[:, None] * inverse[None, :]
    angles = angles.reshape((angles.shape[0],) + (1,) * (values.ndim - 2) + (halfway,))
    cosine_values = jnp.cos(angles)
    sine_values = jnp.sin(angles)
    first_half = values[..., :halfway]
    second_half = values[..., halfway:]
    return jnp.concatenate(
        [
            first_half * cosine_values - second_half * sine_values,
            second_half * cosine_values + first_half * sine_values,
        ],
        axis=-1,
    )


def rms_scale(values, gain_values):
    return (
        values
        * lax.rsqrt(jnp.mean(values * values, axis=-1, keepdims=True) + epsilon)
        * gain_values
    )


def expand(latent_rows, latent_gain, key_up, value_up):
    normed = rms_scale(latent_rows.astype(jnp.float32), latent_gain).astype(jnp.bfloat16)
    keys_nope = jnp.dot(normed, key_up, preferred_element_type=jnp.float32).astype(jnp.bfloat16)
    values = jnp.dot(normed, value_up, preferred_element_type=jnp.float32).astype(jnp.bfloat16)
    lead = latent_rows.shape[:2]
    return (
        keys_nope.reshape(lead + (key_up.shape[1] // NOPE, NOPE)),
        values.reshape(lead + (value_up.shape[1] // VDIM, VDIM)),
    )


def absorb(carried, query_nope, query_rot, key_nope, value_rows, key_rot):
    running, totals, accumulated = carried
    scores = jnp.einsum("qshd,kshd->qshk", query_nope, key_nope, preferred_element_type=jnp.float32)
    scores = scores + jnp.einsum(
        "qshd,ksd->qshk", query_rot, key_rot, preferred_element_type=jnp.float32
    )
    scores = scores * QK ** (-0.5)
    highest = jnp.maximum(running, jnp.max(scores, axis=-1))
    weights = jnp.exp(scores - highest[..., None])
    totals = jnp.sum(weights, axis=-1)
    accumulated = jnp.einsum(
        "qshk,kshd->qshd",
        weights.astype(jnp.bfloat16),
        value_rows,
        preferred_element_type=jnp.float32,
    )
    return (highest, totals, accumulated)


def slots(chosen, row_count, experts_total):
    capacity = max(2, 3 * row_count * TOPK // (2 * experts_total))
    capacity = -(-capacity // 8) * 8
    one_hot = (chosen[:, None] == jnp.arange(experts_total, dtype=jnp.int32)[None, :]).astype(
        jnp.bfloat16
    )
    order = jnp.arange(chosen.shape[0])
    earlier = (order[:, None] > order[None, :]).astype(jnp.bfloat16)
    before = jnp.dot(earlier, one_hot, preferred_element_type=jnp.float32)
    slot_index = jnp.sum(before * one_hot.astype(jnp.float32), axis=-1).astype(jnp.int32)
    return (capacity, chosen * capacity + slot_index)


def whole_out_weight(out_weight):
    pieces = lax.axis_size("sp")
    depth = out_weight.shape[0] // pieces
    own = lax.dynamic_slice_in_dim(out_weight, lax.axis_index("sp") * depth, depth, axis=0)
    return lax.all_gather(own, ("tp", "sp"), axis=0, tiled=True)


def shards(
    residual,
    query,
    latent,
    rope_key,
    latent_gain,
    key_up,
    value_up,
    out_weight,
    norm_gain,
    group_prob,
    pair_logits,
    routes,
    w_gate,
    w_up,
    w_down,
):
    positions_here = query.shape[0]
    heads_here = key_up.shape[1] // NOPE
    own_positions = lax.axis_index("sp") * positions_here + jnp.arange(
        positions_here, dtype=jnp.int32
    )
    split_query = query.reshape(positions_here, SEQS, heads_here, QK)
    query_nope = split_query[..., :NOPE]
    query_rot = rotate(split_query[..., NOPE:].astype(jnp.float32), own_positions).astype(
        jnp.bfloat16
    )
    key_rot = rotate(rope_key.astype(jnp.float32), own_positions).astype(jnp.bfloat16)
    initial = (
        jnp.full((positions_here, SEQS, heads_here), lowest, jnp.float32),
        jnp.zeros((positions_here, SEQS, heads_here), jnp.float32),
        jnp.zeros((positions_here, SEQS, heads_here, VDIM), jnp.float32),
    )
    key_nope, value_rows = expand(
        lax.all_gather(latent, "sp", axis=0, tiled=True), latent_gain, key_up, value_up
    )
    finished = absorb(
        initial,
        query_nope,
        query_rot,
        key_nope,
        value_rows,
        lax.all_gather(key_rot, "sp", axis=0, tiled=True),
    )
    attended = (finished[2] / finished[1][..., None]).astype(jnp.bfloat16)
    attended = attended.reshape(positions_here, SEQS, heads_here * VDIM)
    by_token = lax.all_to_all(attended, "tp", split_axis=0, concat_axis=2, tiled=True)
    row_count = by_token.shape[0] * SEQS
    mixed_heads = by_token.reshape(row_count, by_token.shape[2])
    projected = jnp.dot(
        mixed_heads, whole_out_weight(out_weight), preferred_element_type=jnp.float32
    )
    stream = (residual.reshape(row_count, D).astype(jnp.float32) + projected).astype(jnp.bfloat16)
    normed = rms_scale(stream.astype(jnp.float32), norm_gain).astype(jnp.bfloat16)
    mixing = jax.nn.softmax(pair_logits.reshape(row_count, TOPK), axis=-1) * group_prob.reshape(
        row_count, 1
    )
    experts_total = lax.axis_size("sp") * lax.axis_size("tp")
    capacity, target = slots(routes.reshape(row_count * TOPK), row_count, experts_total)
    spots = target.reshape(row_count, TOPK)
    places = jnp.arange(experts_total * capacity, dtype=jnp.int32)
    picked = spots[:, :, None] == places[None, None, :]
    pick_rows = jnp.any(picked, axis=1).astype(jnp.bfloat16)
    outgoing = lax.dot_general(
        pick_rows, normed, (((0,), (0,)), ((), ())), preferred_element_type=jnp.float32
    ).astype(jnp.bfloat16)
    outgoing = outgoing.reshape(experts_total, capacity, D)
    arrived = lax.all_to_all(outgoing, ("sp", "tp"), split_axis=0, concat_axis=0, tiled=True)
    flat_rows = arrived.reshape(-1, D)
    gate_pre = jnp.dot(flat_rows, w_gate[0], preferred_element_type=jnp.float32)
    upward = jnp.dot(flat_rows, w_up[0], preferred_element_type=jnp.float32)
    hidden = (jax.nn.silu(gate_pre) * upward).astype(jnp.bfloat16)
    served = (
        jnp.dot(hidden, w_down[0], preferred_element_type=jnp.float32)
        .astype(jnp.bfloat16)
        .reshape(arrived.shape)
    )
    returned = lax.all_to_all(served, ("sp", "tp"), split_axis=0, concat_axis=0, tiled=True)
    returned = returned.reshape(experts_total * capacity, D)
    combined = stream.astype(jnp.float32)
    for choice in range(TOPK):
        combined = combined + mixing[:, choice, None] * jnp.dot(
            picked[:, choice].astype(jnp.bfloat16), returned, preferred_element_type=jnp.float32
        )
    return combined.astype(jnp.bfloat16).reshape(residual.shape)


def solution(mesh):
    placed = (
        P(("sp", "tp"), "grp", None),
        P("sp", "grp", "tp"),
        P("sp", "grp", None),
        P("sp", "grp", None),
        P(),
        P(None, "tp"),
        P(None, "tp"),
        P("tp", None),
        P(),
        P(("sp", "tp"), "grp"),
        P(("sp", "tp"), "grp", None),
        P(("sp", "tp"), "grp", None),
        P(("sp", "tp"), None, None),
        P(("sp", "tp"), None, None),
        P(("sp", "tp"), None, None),
    )
    return jax.shard_map(
        shards, mesh=mesh, in_specs=placed, out_specs=P(("sp", "tp"), "grp", None), check_vma=False
    )
```

profile of v0, /device:TPU:0, one launch (start us, length us, event | category | flops | bytes accessed | tf_op | source)
XLA Modules:
  0.0 262.8 jit_solution(14248461183122850936)
XLA Ops:
  7.3 1.9 constant_dynamic-slice_fusion
  9.2 2.0 copy.68
  11.2 3.2 %reshape.201 = bf16[192,4,2,192]{3,2,0,1:T(2,128)(2,1)} reshape(bf16[192,4,384]{2,0,1:T(8,128)(2,1)} %copy.68) | data formatting | bytes 1179648 | tf_op jit(solution)/shard_map/reshape | solution.py:115
  14.4 1.3 slice.43
  16.6 1.9 convert_element_type.90
  18.5 1.8 copy.71
  22.1 1.5 copy.73
  23.6 1.5 copy.72
  25.1 1.3 subtract_convert_fusion
  26.8 14.9 %all_gather.10 = bf16[768,4,64]{2,1,0:T(4,128)(2,1)} all-gather(bf16[192,4,64]{2,1,0:T(4,128)(2,1)S(1)} %pad_maximum_fusion), channel_id=1, replica_groups=mesh['grp'=2,'sp'=4,'tp'=4] {'sp'}, dimensions={0}, use_global_device_ids=true | all-gather | bytes 491520 | tf_op jit(solution)/shard_map/all_gather | solution.py:135
  41.8 2.6 all-gather.3.cloned.1.call-done
  44.4 3.0 %fusion = f32[768,4]{0,1:T(4,128)S(1)} fusion(bf16[768,4,512]{2,1,0:T(4,128)(2,1)} %all-gather.3.cloned.1.call-done), kind=kLoop, calls=%fused_computation.2 | loop fusion | flops 4715520 | bytes 3158016 | tf_op jit(solution)/shard_map/reduce_sum | solution.py:38
  47.4 3.2 %fusion.26 = bf16[768,4,256]{0,2,1:T(8,128)(2,1)S(1)} fusion(f32[512]{0:T(512)S(1)} %copy-done.16, f32[768,4]{0,1:T(4,128)S(1)} %add_rsqrt_fusion, bf16[768,4,512]{2,1,0:T(4,128)(2,1)S(1)} %copy-done.2, bf16[512,256]{1,0:T(8,128)(2,1)} %param.20), kind=kOutput, calls=%fused_computation.31 | convolution fusion | flops 812384256 | bytes 4995072 | tf_op jit(solution)/shard_map/dot_general | solution.py:45
  52.7 1.3 fusion.4
  54.0 2.2 fusion.23
  56.3 1.2 fusion.38
  58.9 4.6 %all-to-all-start = ((bf16[192,4,256]{2,1,0:T(4,128)(2,1)}), bf16[192,4,256]{2,1,0:T(4,128)(2,1)S(1)}, u32[]{:S(2)}, u32[]{:S(2)}) async-start(bf16[192,4,256]{2,1,0:T(4,128)(2,1)} %reshape.214), calls=%async_computation | async-start | bytes 786432 | tf_op jit(solution)/shard_map/all_to_all | solution.py:139
  63.5 2.5 reshape.210
  68.3 1.0 eq.28
  71.4 1.7 iota_compare_fusion
  73.0 3.5 %all-to-all-done = bf16[192,4,256]{2,1,0:T(4,128)(2,1)S(1)} async-done(((bf16[192,4,256]{2,1,0:T(4,128)(2,1)}), bf16[192,4,256]{2,1,0:T(4,128)(2,1)S(1)}, u32[]{:S(2)}, u32[]{:S(2)}) %all-to-all-start) | async-done | bytes 393248 | tf_op jit(solution)/shard_map/all_to_all | solution.py:139
  77.0 21.5 %all-gather.5.cloned.1.call-done = bf16[1024,2048]{1,0:T(8,128)(2,1)} async-done(((bf16[64,2048]{1,0:T(8,128)(2,1)}), bf16[1024,2048]{1,0:T(8,128)(2,1)}) %all-gather.5.cloned.1.call-update) | async-done | bytes 4194320 | tf_op jit(solution)/shard_map/all_gather | solution.py:90
  98.5 3.8 %multiply_reduce_fusion = (f32[192]{0:T(256)S(1)}, f32[192,2048]{1,0:T(8,128)S(1)}) fusion(f32[192,2048]{1,0:T(8,128)} %reshape.210, bf16[192,1024]{1,0:T(8,128)(2,1)S(1)} %bitcast.72, bf16[1024,2048]{1,0:T(8,128)(2,1)} %all-gather.5.cloned.1.call-done), kind=kOutput, calls=%fused_computation.33 | convolution fusion | flops 807272256 | bytes 7734016 | tf_op jit(solution)/shard_map/dot_general | solution.py:142
  103.3 63.9 %all_to_all.25 = bf16[16,40,2048]{2,1,0:T(8,128)(2,1)S(1)} all-to-all(bf16[16,40,2048]{2,1,0:T(8,128)(2,1)S(1)} %bitcast.66), channel_id=1, replica_groups=mesh['grp'=2,'sp'=4,'tp'=4] {'sp','tp'}, dimensions={0} | all-to-all | bytes 5242880 | tf_op jit(solution)/shard_map/all_to_all | solution.py:160
  167.2 1.5 copy-done.4
  168.7 3.5 %fusion.9 = f32[640,768]{1,0:T(8,128)} fusion(bf16[640,2048]{1,0:T(8,128)(2,1)S(1)} %bitcast.70, bf16[1,2048,768]{2,1,0:T(8,128)(2,1)S(1)} %copy-done.14), kind=kOutput, calls=%fused_computation.15 | convolution fusion | flops 2013265920 | bytes 7733248 | tf_op jit(solution)/shard_map/dot_general | solution.py:162
  172.2 9.7 %convolution_convert_fusion = bf16[640,2048]{1,0:T(8,128)(2,1)} fusion(bf16[1,768,2048]{2,1,0:T(8,128)(2,1)S(1)} %copy-done, f32[640,768]{1,0:T(8,128)} %fusion.9, bf16[640,2048]{1,0:T(8,128)(2,1)} %bitcast.71, bf16[1,2048,768]{2,1,0:T(8,128)(2,1)} %param.28), kind=kOutput, calls=%fused_computation.10 | convolution fusion | flops 4030791680 | bytes 13500416 | tf_op jit(solution)/shard_map/dot_general | solution.py:166
  181.9 4.6 %all-to-all-start.2 = ((bf16[16,40,2048]{2,1,0:T(8,128)(2,1)}), bf16[16,40,2048]{2,1,0:T(8,128)(2,1)}, u32[]{:S(2)}, u32[]{:S(2)}) async-start(bf16[16,40,2048]{2,1,0:T(8,128)(2,1)} %bitcast.69), calls=%async_computation.2 | async-start | bytes 5242880 | tf_op jit(solution)/shard_map/all_to_all | solution.py:170
  187.4 59.7 %all-to-all-done.2 = bf16[16,40,2048]{2,1,0:T(8,128)(2,1)} async-done(((bf16[16,40,2048]{2,1,0:T(8,128)(2,1)}), bf16[16,40,2048]{2,1,0:T(8,128)(2,1)}, u32[]{:S(2)}, u32[]{:S(2)}) %all-to-all-start.2) | async-done | bytes 2621472 | tf_op jit(solution)/shard_map/all_to_all | solution.py:170
  247.1 3.0 %fusion.12 = f32[192,2048]{1,0:T(8,128)S(1)} fusion(f32[192,2048]{1,0:T(8,128)} %copy-done.1, bf16[640,2048]{1,0:T(8,128)(2,1)} %bitcast.18, f32[192]{0:T(256)S(1)} %bitcast.75, pred[192,2,640]{2,0,1:T(32,128)(4,1)S(1)} %copy-done.6), kind=kOutput, calls=%fused_computation.21 | convolution fusion | flops 504102912 | bytes 5891072 | tf_op jit(solution)/shard_map/dot_general | solution.py:174
  250.1 3.5 %fusion.13 = bf16[192,2048]{1,0:T(8,128)(2,1)} fusion(f32[192,2048]{1,0:T(8,128)S(1)} %fusion.12, bf16[640,2048]{1,0:T(8,128)(2,1)} %bitcast.18, f32[192]{0:T(256)S(1)} %bitcast.76, pred[192,2,640]{2,0,1:T(32,128)(4,1)S(1)} %copy-done.6), kind=kOutput, calls=%fused_computation.22 | convolution fusion | flops 504496128 | bytes 5104640 | tf_op jit(solution)/shard_map/dot_general | solution.py:174
  253.6 2.4 reshape.209
  (77 shorter events, 14.1 us)
Async XLA Ops:
  6.5 165.7 %copy-start = (bf16[1,768,2048]{2,1,0:T(8,128)(2,1)S(1)}, bf16[1,768,2048]{2,1,0:T(8,128)(2,1)}, u32[]{:S(2)}) copy-start(bf16[1,768,2048]{2,1,0:T(8,128)(2,1)} %param.29) | copy-start | bytes 9437188
  6.5 37.8 %all-gather.3.cloned.1.call-start = ((), (), s32[]{:S(2)}) async-start(), calls=%async_computation.3 | async-start | bytes 3932160 | tf_op jit(solution)/shard_map/all_gather | solution.py:127
  7.3 91.2 %all-gather.5.cloned.1.call-start = ((), (), s32[]{:S(2)}) async-start(), calls=%async_computation.4 | async-start | bytes 4456448 | tf_op jit(solution)/shard_map/all_gather | solution.py:90
  25.1 16.6 %copy-start.5 = (f32[192,4,2,64]{0,3,2,1:T(8,128)S(1)}, f32[192,4,2,64]{0,3,2,1:T(8,128)}, u32[]{:S(2)}) copy-start(f32[192,4,2,64]{0,3,2,1:T(8,128)} %convert_element_type.90) | copy-start | bytes 1179652
  25.1 16.6 %copy-start.8 = (f32[192,32]{0,1:T(8,128)S(1)}, f32[192,32]{0,1:T(8,128)}, u32[]{:S(2)}) copy-start(f32[192,32]{0,1:T(8,128)} %get-tuple-element.13) | copy-start | bytes 73732
  25.1 16.6 %copy-start.9 = (f32[192,32]{0,1:T(8,128)S(1)}, f32[192,32]{0,1:T(8,128)}, u32[]{:S(2)}) copy-start(f32[192,32]{0,1:T(8,128)} %get-tuple-element.14) | copy-start | bytes 73732
  26.8 20.6 %copy-start.16 = (f32[512]{0:T(512)S(1)}, f32[512]{0:T(512)}, u32[]{:S(2)}) copy-start(f32[512]{0:T(512)} %param.19) | copy-start | bytes 6148
  44.4 3.0 %copy-start.2 = (bf16[768,4,512]{2,1,0:T(4,128)(2,1)S(1)}, bf16[768,4,512]{2,1,0:T(4,128)(2,1)}, u32[]{:S(2)}) copy-start(bf16[768,4,512]{2,1,0:T(4,128)(2,1)} %all-gather.3.cloned.1.call-done) | copy-start | bytes 9437188
  47.4 3.2 %slice-start = ((bf16[192,4,2,192]{3,2,0,1:T(2,128)(2,1)}), bf16[192,4,2,128]{3,2,0,1:T(2,128)(2,1)S(1)}, s32[]{:S(2)}) async-start(bf16[192,4,2,192]{3,2,0,1:T(2,128)(2,1)} %reshape.201), calls=%async_computation.5 | async-start | bytes 786432 | tf_op jit(solution)/shard_map/slice | solution.py:116
  50.6 1.1 copy-start.3
  52.7 1.3 copy-start.15
  57.4 8.5 %copy-start.11 = (s32[48,4,2]{0,2,1:T(2,128)S(1)}, s32[48,4,2]{0,2,1:T(2,128)}, u32[]{:S(2)}) copy-start(s32[48,4,2]{0,2,1:T(2,128)} %param.26) | copy-start | bytes 4612
  58.9 17.7 %all-to-all-start = ((bf16[192,4,256]{2,1,0:T(4,128)(2,1)}), bf16[192,4,256]{2,1,0:T(4,128)(2,1)S(1)}, u32[]{:S(2)}, u32[]{:S(2)}) async-start(bf16[192,4,256]{2,1,0:T(4,128)(2,1)} %reshape.214), calls=%async_computation | async-start | bytes 786432 | tf_op jit(solution)/shard_map/all_to_all | solution.py:139
  98.5 3.8 %copy-start.7 = (pred[192,640]{1,0:T(8,128)(4,1)S(1)}, pred[192,640]{1,0:T(8,128)(4,1)}, u32[]{:S(2)}) copy-start(pred[192,640]{1,0:T(8,128)(4,1)} %get-tuple-element.12) | copy-start | bytes 368644
  98.5 3.8 %copy-start.12 = (f32[2048]{0:T(1024)S(1)}, f32[2048]{0:T(1024)}, u32[]{:S(2)}) copy-start(f32[2048]{0:T(1024)} %param.23) | copy-start | bytes 24580
  102.3 64.9 %copy-start.1 = (f32[192,2048]{1,0:T(8,128)}, f32[192,2048]{1,0:T(8,128)S(1)}, u32[]{:S(2)}) copy-start(f32[192,2048]{1,0:T(8,128)S(1)} %get-tuple-element.18) | copy-start | bytes 4718596
  103.3 65.4 %copy-start.14 = (bf16[1,2048,768]{2,1,0:T(8,128)(2,1)S(1)}, bf16[1,2048,768]{2,1,0:T(8,128)(2,1)}, u32[]{:S(2)}) copy-start(bf16[1,2048,768]{2,1,0:T(8,128)(2,1)} %param.27) | copy-start | bytes 9437188
  167.2 1.5 copy-start.4
  181.9 4.6 %copy-start.10 = (f32[48,4,2]{0,2,1:T(2,128)S(1)}, f32[48,4,2]{0,2,1:T(2,128)}, u32[]{:S(2)}) copy-start(f32[48,4,2]{0,2,1:T(2,128)} %param.25) | copy-start | bytes 4612
  181.9 4.8 %copy-start.13 = (f32[48,4]{0,1:T(4,128)S(1)}, f32[48,4]{0,1:T(4,128)}, u32[]{:S(2)}) copy-start(f32[48,4]{0,1:T(4,128)} %param.24) | copy-start | bytes 2308
  181.9 65.2 %copy-start.6 = (pred[192,2,640]{2,0,1:T(32,128)(4,1)S(1)}, pred[192,2,640]{2,0,1:T(32,128)(4,1)}, u32[]{:S(2)}) copy-start(pred[192,2,640]{2,0,1:T(32,128)(4,1)} %get-tuple-element.11) | copy-start | bytes 737284
  181.9 65.2 %all-to-all-start.2 = ((bf16[16,40,2048]{2,1,0:T(8,128)(2,1)}), bf16[16,40,2048]{2,1,0:T(8,128)(2,1)}, u32[]{:S(2)}, u32[]{:S(2)}) async-start(bf16[16,40,2048]{2,1,0:T(8,128)(2,1)} %bitcast.69), calls=%async_computation.2 | async-start | bytes 5242880 | tf_op jit(solution)/shard_map/all_to_all | solution.py:170
Sparse Core Ops, SparseCore 0:
  8.9 35.4 all-gather.2
  46.5 51.8 all-gather.4
where the time goes:
time: 264 us; the launch traced here: 263 us
  waiting for transfers between devices  88 us (33%)
  blocking collectives  78.8 us (30%)
  matrix products  33 us (12%)
  local copies, waits for them, and re-layouts  28.6 us (11%)
  between operations  13.7 us (5%)
  other arithmetic  11.4 us (4%)
  starting transfers between devices  9.24 us (4%)
    all_to_all x1, blocking collectives, shards(): lax.all_to_all(outgoing, ('sp', 'tp'), split_axis=0, concat_axis=0, tiled...  63.9 us
    all_to_all x1, waiting for transfers between devices, shards(): lax.all_to_all(served, ('sp', 'tp'), split_axis=0, concat_axis=0, tiled=T...  59.7 us
    all_gather x1, waiting for transfers between devices, whole_out_weight(): return lax.all_gather(own, ('tp', 'sp'), axis=0, tiled=True)  21.5 us
    all_gather x1, blocking collectives, shards(): lax.all_gather(key_rot, 'sp', axis=0, tiled=True)  14.9 us
    dot_general x1, matrix products, shards(): jnp.dot(hidden, w_down[0], preferred_element_type=jnp.float32)  9.66 us
    unnamed x41, local copies, waits for them, and re-layouts  7.63 us
    dot_general x2, matrix products, shards(): jnp.dot(picked[:, choice].astype(jnp.bfloat16), returned, preferred_eleme...  6.52 us
  transfers between devices with their start and end apart: 4, of which 4 were waited for; matrix products, arithmetic and copies ran while one was open for 17% of the time, Pallas kernels for 0%

commit v1 on v0

--- a/solution.py
+++ b/solution.py
@@ -12,6 +12,18 @@
 epsilon = 1e-06
 rotary_base = 10000.0
 lowest = -1e30
+
+
+def sent_to_each(value, axis, split, join):
+    ways, here = (lax.axis_size(axis), lax.axis_index(axis))
+    width = value.shape[split] // ways
+    turned = jnp.roll(value, -here * width, axis=split)
+    got = [lax.slice_in_dim(turned, 0, width, axis=split)]
+    for far in range(1, ways):
+        sent = lax.slice_in_dim(turned, far * width, (far + 1) * width, axis=split)
+        got.append(lax.ppermute(sent, axis, [(d, (d + far) % ways) for d in range(ways)]))
+    line = jnp.concatenate(got[::-1], axis=join)
+    return jnp.roll(line, (here + 1) * got[0].shape[join], axis=join)
 
 
 def rotate(values, positions):
@@ -157,7 +169,7 @@
         pick_rows, normed, (((0,), (0,)), ((), ())), preferred_element_type=jnp.float32
     ).astype(jnp.bfloat16)
     outgoing = outgoing.reshape(experts_total, capacity, D)
-    arrived = lax.all_to_all(outgoing, ("sp", "tp"), split_axis=0, concat_axis=0, tiled=True)
+    arrived = sent_to_each(outgoing, ("sp", "tp"), 0, 0)
     flat_rows = arrived.reshape(-1, D)
     gate_pre = jnp.dot(flat_rows, w_gate[0], preferred_element_type=jnp.float32)
     upward = jnp.dot(flat_rows, w_up[0], preferred_element_type=jnp.float32)

time: 264 us -> 266 us (level)
  blocking collectives: 78.8 us -> 14.9 us
  waiting for transfers between devices: 88 us -> 119 us
  starting transfers between devices: 9.24 us -> 38.7 us
  local copies, waits for them, and re-layouts: 28.6 us -> 33.9 us
    all_to_all x1 -> x0, blocking collectives: 63.9 us -> none  [shards(): lax.all_to_all(outgoing, ('sp', 'tp'), split_axis=0, concat_axis=0, tiled...]
    ppermute x0 -> x15, starting transfers between devices: none -> 29.4 us  [sent_to_each(): lax.ppermute(sent, axis, [(d, (d + far) % ways) for d in range(ways)])]
    ppermute x0 -> x15, waiting for transfers between devices: none -> 29 us  [sent_to_each(): lax.ppermute(sent, axis, [(d, (d + far) % ways) for d in range(ways)])]
    unnamed x41 -> x62, local copies, waits for them, and re-layouts: 7.63 us -> 11.5 us
  transfers between devices with their start and end apart: 4 -> 19, of which waited for: 4 -> 8; matrix products, arithmetic and copies ran while one was open for 17% -> 16% of each run, Pallas kernels for 0% -> 0%
where the time goes in v1:
time: 266 us
  waiting for transfers between devices  119 us (45%)
  starting transfers between devices  38.7 us (15%)
  local copies, waits for them, and re-layouts  33.9 us (13%)
  matrix products  33 us (12%)
  blocking collectives  14.9 us (6%)
  between operations  13.9 us (5%)
  other arithmetic  11.7 us (4%)
    all_to_all x1, waiting for transfers between devices, shards(): lax.all_to_all(served, ('sp', 'tp'), split_axis=0, concat_axis=0, tiled=T...  59.7 us
    ppermute x15, starting transfers between devices, sent_to_each(): lax.ppermute(sent, axis, [(d, (d + far) % ways) for d in range(ways)])  29.4 us
    ppermute x15, waiting for transfers between devices, sent_to_each(): lax.ppermute(sent, axis, [(d, (d + far) % ways) for d in range(ways)])  29 us
    all_gather x1, waiting for transfers between devices, whole_out_weight(): return lax.all_gather(own, ('tp', 'sp'), axis=0, tiled=True)  21.5 us
    all_gather x1, blocking collectives, shards(): lax.all_gather(key_rot, 'sp', axis=0, tiled=True)  14.9 us
    unnamed x62, local copies, waits for them, and re-layouts  11.5 us
    dot_general x1, matrix products, shards(): jnp.dot(hidden, w_down[0], preferred_element_type=jnp.float32)  9.66 us
    dot_general x2, matrix products, shards(): jnp.dot(picked[:, choice].astype(jnp.bfloat16), returned, preferred_eleme...  6.51 us
  transfers between devices with their start and end apart: 19, of which 8 were waited for; matrix products, arithmetic and copies ran while one was open for 16% of the time, Pallas kernels for 0%

profile of v1, /device:TPU:0, one launch (start us, length us, event | category | flops | bytes accessed | tf_op | source)
XLA Modules:
  0.0 265.5 jit_solution(4109160225791945205)
XLA Ops:
  9.2 2.0 copy.68
  11.2 3.2 %reshape.201 = bf16[192,4,2,192]{3,2,0,1:T(2,128)(2,1)} reshape(bf16[192,4,384]{2,0,1:T(8,128)(2,1)} %copy.68) | data formatting | bytes 1179648 | tf_op jit(solution)/shard_map/reshape | solution.py:127
  14.4 2.0 slice.107
  20.0 1.9 copy.99
  24.5 14.9 %all_gather.10 = bf16[768,4,64]{2,1,0:T(4,128)(2,1)} all-gather(bf16[192,4,64]{2,1,0:T(4,128)(2,1)S(1)} %pad_maximum_fusion), channel_id=1, replica_groups=mesh['grp'=2,'sp'=4,'tp'=4] {'sp'}, dimensions={0}, use_global_device_ids=true | all-gather | bytes 491520 | tf_op jit(solution)/shard_map/all_gather | solution.py:147
  39.5 4.9 %all-gather.3.cloned.1.call-done = bf16[768,4,512]{2,1,0:T(4,128)(2,1)} async-done(((bf16[192,4,512]{2,1,0:T(4,128)(2,1)}), bf16[768,4,512]{2,1,0:T(4,128)(2,1)}) %all-gather.3.cloned.1.call-update) | async-done | bytes 3145744 | tf_op jit(solution)/shard_map/all_gather | solution.py:139
  44.4 3.0 %fusion = f32[768,4]{0,1:T(4,128)S(1)} fusion(bf16[768,4,512]{2,1,0:T(4,128)(2,1)} %all-gather.3.cloned.1.call-done), kind=kLoop, calls=%fused_computation.2 | loop fusion | flops 4715520 | bytes 3158016 | tf_op jit(solution)/shard_map/reduce_sum | solution.py:50
  47.4 3.2 %fusion.28 = bf16[768,4,256]{0,2,1:T(8,128)(2,1)S(1)} fusion(f32[512]{0:T(512)S(1)} %copy-done.19, f32[768,4]{0,1:T(4,128)S(1)} %add_rsqrt_fusion, bf16[768,4,512]{2,1,0:T(4,128)(2,1)S(1)} %copy-done.3, bf16[512,256]{1,0:T(8,128)(2,1)} %param.22), kind=kOutput, calls=%fused_computation.37 | convolution fusion | flops 812384256 | bytes 4995072 | tf_op jit(solution)/shard_map/dot_general | solution.py:57
  54.1 2.2 fusion.25
  58.9 4.5 %all-to-all-start = ((bf16[192,4,256]{2,1,0:T(4,128)(2,1)}), bf16[192,4,256]{2,1,0:T(4,128)(2,1)S(1)}, u32[]{:S(2)}, u32[]{:S(2)}) async-start(bf16[192,4,256]{2,1,0:T(4,128)(2,1)} %reshape.214), calls=%async_computation | async-start | bytes 786432 | tf_op jit(solution)/shard_map/all_to_all | solution.py:151
  63.5 2.5 reshape.210
  73.0 3.6 %all-to-all-done = bf16[192,4,256]{2,1,0:T(4,128)(2,1)S(1)} async-done(((bf16[192,4,256]{2,1,0:T(4,128)(2,1)}), bf16[192,4,256]{2,1,0:T(4,128)(2,1)S(1)}, u32[]{:S(2)}, u32[]{:S(2)}) %all-to-all-start) | async-done | bytes 393248 | tf_op jit(solution)/shard_map/all_to_all | solution.py:151
  77.0 21.5 %all-gather.5.cloned.1.call-done = bf16[1024,2048]{1,0:T(8,128)(2,1)} async-done(((bf16[64,2048]{1,0:T(8,128)(2,1)}), bf16[1024,2048]{1,0:T(8,128)(2,1)}) %all-gather.5.cloned.1.call-update) | async-done | bytes 4194320 | tf_op jit(solution)/shard_map/all_gather | solution.py:102
  98.5 3.8 %multiply_reduce_fusion = (f32[192]{0:T(256)S(1)}, f32[192,2048]{1,0:T(8,128)S(1)}) fusion(f32[192,2048]{1,0:T(8,128)} %reshape.210, bf16[192,1024]{1,0:T(8,128)(2,1)S(1)} %bitcast.72, bf16[1024,2048]{1,0:T(8,128)(2,1)} %all-gather.5.cloned.1.call-done), kind=kOutput, calls=%fused_computation.39 | convolution fusion | flops 807272256 | bytes 7734016 | tf_op jit(solution)/shard_map/dot_general | solution.py:154
  112.9 3.1 %collective-permute-start.4 = (bf16[1,40,2048]{2,1,0:T(8,128)(2,1)}, bf16[1,40,2048]{2,1,0:T(8,128)(2,1)S(1)}, u32[]{:S(2)}, u32[]{:S(2)}) collective-permute-start(bf16[1,40,2048]{2,1,0:T(8,128)(2,1)} %get-tuple-element.16), channel_id=1, source_target_pairs={{0,11},{1,12},{2,13},{3,14},{4,15},{5,0},{6,1},{7,2},{8,3},{9,4},{... | collective-permute-start | bytes 491528 | tf_op jit(solution)/shard_map/ppermute | solution.py:24
  118.4 12.2 %collective-permute-done.1 = bf16[1,40,2048]{2,1,0:T(8,128)(2,1)S(1)} collective-permute-done((bf16[1,40,2048]{2,1,0:T(8,128)(2,1)}, bf16[1,40,2048]{2,1,0:T(8,128)(2,1)S(1)}, u32[]{:S(2)}, u32[]{:S(2)}) %collective-permute-start.1) | collective-permute-done | bytes 163872 | tf_op jit(solution)/shard_map/ppermute | solution.py:24
  131.3 3.3 %collective-permute-start.8 = (bf16[1,40,2048]{2,1,0:T(8,128)(2,1)}, bf16[1,40,2048]{2,1,0:T(8,128)(2,1)S(1)}, u32[]{:S(2)}, u32[]{:S(2)}) collective-permute-start(bf16[1,40,2048]{2,1,0:T(8,128)(2,1)} %get-tuple-element.12), channel_id=1, source_target_pairs={{0,7},{1,8},{2,9},{3,10},{4,11},{5,12},{6,13},{7,14},{8,15},{9,0},... | collective-permute-start | bytes 491528 | tf_op jit(solution)/shard_map/ppermute | solution.py:24
  134.6 2.3 collective-permute-start.9
  136.9 2.8 %collective-permute-done.5 = bf16[1,40,2048]{2,1,0:T(8,128)(2,1)S(1)} collective-permute-done((bf16[1,40,2048]{2,1,0:T(8,128)(2,1)}, bf16[1,40,2048]{2,1,0:T(8,128)(2,1)S(1)}, u32[]{:S(2)}, u32[]{:S(2)}) %collective-permute-start.5) | collective-permute-done | bytes 163872 | tf_op jit(solution)/shard_map/ppermute | solution.py:24
  139.7 3.9 %collective-permute-start.10 = (bf16[1,40,2048]{2,1,0:T(8,128)(2,1)}, bf16[1,40,2048]{2,1,0:T(8,128)(2,1)S(1)}, u32[]{:S(2)}, u32[]{:S(2)}) collective-permute-start(bf16[1,40,2048]{2,1,0:T(8,128)(2,1)} %get-tuple-element.10), channel_id=1, source_target_pairs={{0,5},{1,6},{2,7},{3,8},{4,9},{5,10},{6,11},{7,12},{8,13},{9,14},{... | collective-permute-start | bytes 491528 | tf_op jit(solution)/shard_map/ppermute | solution.py:24
  144.1 2.9 %collective-permute-start.12 = (bf16[1,40,2048]{2,1,0:T(8,128)(2,1)}, bf16[1,40,2048]{2,1,0:T(8,128)(2,1)S(1)}, u32[]{:S(2)}, u32[]{:S(2)}) collective-permute-start(bf16[1,40,2048]{2,1,0:T(8,128)(2,1)} %get-tuple-element.8), channel_id=1, source_target_pairs={{0,3},{1,4},{2,5},{3,6},{4,7},{5,8},{6,9},{7,10},{8,11},{9,12},{10... | collective-permute-start | bytes 491528 | tf_op jit(solution)/shard_map/ppermute | solution.py:24
  147.0 3.8 %collective-permute-start.13 = (bf16[1,40,2048]{2,1,0:T(8,128)(2,1)S(1)}, bf16[1,40,2048]{2,1,0:T(8,128)(2,1)S(1)}, u32[]{:S(2)}, u32[]{:S(2)}) collective-permute-start(bf16[1,40,2048]{2,1,0:T(8,128)(2,1)S(1)} %get-tuple-element.7), channel_id=1, source_target_pairs={{0,2},{1,3},{2,4},{3,5},{4,6},{5,7},{6,8},{7,9},{8,10},{9,11},{10,... | collective-permute-start | bytes 491528 | tf_op jit(solution)/shard_map/ppermute | solution.py:24
  150.9 4.4 %collective-permute-done.9 = bf16[1,40,2048]{2,1,0:T(8,128)(2,1)S(1)} collective-permute-done((bf16[1,40,2048]{2,1,0:T(8,128)(2,1)}, bf16[1,40,2048]{2,1,0:T(8,128)(2,1)S(1)}, u32[]{:S(2)}, u32[]{:S(2)}) %collective-permute-start.9) | collective-permute-done | bytes 163872 | tf_op jit(solution)/shard_map/ppermute | solution.py:24
  155.3 2.9 %collective-permute-start.14 = (bf16[1,40,2048]{2,1,0:T(8,128)(2,1)S(1)}, bf16[1,40,2048]{2,1,0:T(8,128)(2,1)S(1)}, u32[]{:S(2)}, u32[]{:S(2)}) collective-permute-start(bf16[1,40,2048]{2,1,0:T(8,128)(2,1)S(1)} %get-tuple-element.6), channel_id=1, source_target_pairs={{0,1},{1,2},{2,3},{3,4},{4,5},{5,6},{6,7},{7,8},{8,9},{9,10},{10,1... | collective-permute-start | bytes 491528 | tf_op jit(solution)/shard_map/ppermute | solution.py:24
  158.3 9.6 %collective-permute-done.13 = bf16[1,40,2048]{2,1,0:T(8,128)(2,1)S(1)} collective-permute-done((bf16[1,40,2048]{2,1,0:T(8,128)(2,1)S(1)}, bf16[1,40,2048]{2,1,0:T(8,128)(2,1)S(1)}, u32[]{:S(2)}, u32[]{:S(2)}) %collective-permute-start.13) | collective-permute-done | bytes 163872 | tf_op jit(solution)/shard_map/ppermute | solution.py:24
  171.3 3.5 %fusion.9 = f32[640,768]{1,0:T(8,128)} fusion(bf16[640,2048]{1,0:T(8,128)(2,1)S(1)} %bitcast.70, bf16[1,2048,768]{2,1,0:T(8,128)(2,1)S(1)} %copy-done.17), kind=kOutput, calls=%fused_computation.19 | convolution fusion | flops 2013265920 | bytes 7733248 | tf_op jit(solution)/shard_map/dot_general | solution.py:174
  174.8 9.7 %convolution_convert_fusion = bf16[640,2048]{1,0:T(8,128)(2,1)} fusion(bf16[1,768,2048]{2,1,0:T(8,128)(2,1)S(1)} %copy-done, f32[640,768]{1,0:T(8,128)} %fusion.9, bf16[640,2048]{1,0:T(8,128)(2,1)} %bitcast.71, bf16[1,2048,768]{2,1,0:T(8,128)(2,1)} %param.30), kind=kOutput, calls=%fused_computation.14 | convolution fusion | flops 4030791680 | bytes 13500416 | tf_op jit(solution)/shard_map/dot_general | solution.py:178
  184.5 4.6 %all-to-all-start.1 = ((bf16[16,40,2048]{2,1,0:T(8,128)(2,1)}), bf16[16,40,2048]{2,1,0:T(8,128)(2,1)}, u32[]{:S(2)}, u32[]{:S(2)}) async-start(bf16[16,40,2048]{2,1,0:T(8,128)(2,1)} %bitcast.69), calls=%async_computation.1 | async-start | bytes 5242880 | tf_op jit(solution)/shard_map/all_to_all | solution.py:182
  190.1 59.7 %all-to-all-done.1 = bf16[16,40,2048]{2,1,0:T(8,128)(2,1)} async-done(((bf16[16,40,2048]{2,1,0:T(8,128)(2,1)}), bf16[16,40,2048]{2,1,0:T(8,128)(2,1)}, u32[]{:S(2)}, u32[]{:S(2)}) %all-to-all-start.1) | async-done | bytes 2621472 | tf_op jit(solution)/shard_map/all_to_all | solution.py:182
  249.8 3.0 %fusion.14 = f32[192,2048]{1,0:T(8,128)S(1)} fusion(f32[192,2048]{1,0:T(8,128)} %copy-done.1, bf16[640,2048]{1,0:T(8,128)(2,1)} %bitcast.18, f32[192]{0:T(256)S(1)} %bitcast.75, pred[192,2,640]{2,0,1:T(32,128)(4,1)S(1)} %copy-done.6), kind=kOutput, calls=%fused_computation.27 | convolution fusion | flops 504102912 | bytes 5891072 | tf_op jit(solution)/shard_map/dot_general | solution.py:186
  252.8 3.5 %fusion.15 = bf16[192,2048]{1,0:T(8,128)(2,1)} fusion(f32[192,2048]{1,0:T(8,128)S(1)} %fusion.14, bf16[640,2048]{1,0:T(8,128)(2,1)} %bitcast.18, f32[192]{0:T(256)S(1)} %bitcast.76, pred[192,2,640]{2,0,1:T(32,128)(4,1)S(1)} %copy-done.6), kind=kOutput, calls=%fused_computation.28 | convolution fusion | flops 504496128 | bytes 5104640 | tf_op jit(solution)/shard_map/dot_general | solution.py:186
  256.3 2.4 reshape.209
  (131 shorter events, 40.8 us)
Async XLA Ops:
  6.5 168.3 %copy-start = (bf16[1,768,2048]{2,1,0:T(8,128)(2,1)S(1)}, bf16[1,768,2048]{2,1,0:T(8,128)(2,1)}, u32[]{:S(2)}) copy-start(bf16[1,768,2048]{2,1,0:T(8,128)(2,1)} %param.31) | copy-start | bytes 9437188
  6.5 37.9 %all-gather.3.cloned.1.call-start = ((), (), s32[]{:S(2)}) async-start(), calls=%async_computation.2 | async-start | bytes 3932160 | tf_op jit(solution)/shard_map/all_gather | solution.py:139
  7.3 91.2 %all-gather.5.cloned.1.call-start = ((), (), s32[]{:S(2)}) async-start(), calls=%async_computation.3 | async-start | bytes 4456448 | tf_op jit(solution)/shard_map/all_gather | solution.py:102
  7.3 10.9 %copy-start.12 = (bf16[192,4,64]{0,2,1:T(8,128)(2,1)S(1)}, bf16[192,4,64]{0,2,1:T(8,128)(2,1)}, u32[]{:S(2)}) copy-start(bf16[192,4,64]{0,2,1:T(8,128)(2,1)} %param.20) | copy-start | bytes 294916
  21.9 17.5 %copy-start.9 = (f32[192,32]{0,1:T(8,128)S(1)}, f32[192,32]{0,1:T(8,128)}, u32[]{:S(2)}) copy-start(f32[192,32]{0,1:T(8,128)} %copy-done.8) | copy-start | bytes 73732
  21.9 17.5 %copy-start.11 = (f32[192,32]{0,1:T(8,128)S(1)}, f32[192,32]{0,1:T(8,128)}, u32[]{:S(2)}) copy-start(f32[192,32]{0,1:T(8,128)} %copy-done.10) | copy-start | bytes 73732
  24.5 22.9 %copy-start.19 = (f32[512]{0:T(512)S(1)}, f32[512]{0:T(512)}, u32[]{:S(2)}) copy-start(f32[512]{0:T(512)} %param.21) | copy-start | bytes 6148
  44.4 3.0 %copy-start.3 = (bf16[768,4,512]{2,1,0:T(4,128)(2,1)S(1)}, bf16[768,4,512]{2,1,0:T(4,128)(2,1)}, u32[]{:S(2)}) copy-start(bf16[768,4,512]{2,1,0:T(4,128)(2,1)} %all-gather.3.cloned.1.call-done) | copy-start | bytes 9437188
  47.4 3.2 %slice-start = ((bf16[192,4,2,192]{3,2,0,1:T(2,128)(2,1)}), bf16[192,4,2,128]{3,2,0,1:T(2,128)(2,1)S(1)}, s32[]{:S(2)}) async-start(bf16[192,4,2,192]{3,2,0,1:T(2,128)(2,1)} %reshape.201), calls=%async_computation.4 | async-start | bytes 786432 | tf_op jit(solution)/shard_map/slice | solution.py:128
  57.5 8.5 %copy-start.14 = (s32[48,4,2]{0,2,1:T(2,128)S(1)}, s32[48,4,2]{0,2,1:T(2,128)}, u32[]{:S(2)}) copy-start(s32[48,4,2]{0,2,1:T(2,128)} %param.28) | copy-start | bytes 4612
  58.9 17.7 %all-to-all-start = ((bf16[192,4,256]{2,1,0:T(4,128)(2,1)}), bf16[192,4,256]{2,1,0:T(4,128)(2,1)S(1)}, u32[]{:S(2)}, u32[]{:S(2)}) async-start(bf16[192,4,256]{2,1,0:T(4,128)(2,1)} %reshape.214), calls=%async_computation | async-start | bytes 786432 | tf_op jit(solution)/shard_map/all_to_all | solution.py:151
  98.5 5.0 %copy-start.7 = (pred[192,640]{1,0:T(8,128)(4,1)S(1)}, pred[192,640]{1,0:T(8,128)(4,1)}, u32[]{:S(2)}) copy-start(pred[192,640]{1,0:T(8,128)(4,1)} %get-tuple-element.28) | copy-start | bytes 368644
  98.5 5.0 %copy-start.15 = (f32[2048]{0:T(1024)S(1)}, f32[2048]{0:T(1024)}, u32[]{:S(2)}) copy-start(f32[2048]{0:T(1024)} %param.25) | copy-start | bytes 24580
  108.3 7.7 %collective-permute-start = (bf16[1,40,2048]{2,1,0:T(8,128)(2,1)}, bf16[1,40,2048]{2,1,0:T(8,128)(2,1)}, u32[]{:S(2)}, u32[]{:S(2)}) collective-permute-start(bf16[1,40,2048]{2,1,0:T(8,128)(2,1)} %get-tuple-element.20), channel_id=1, source_target_pairs={{0,15},{1,0},{2,1},{3,2},{4,3},{5,4},{6,5},{7,6},{8,7},{9,8},{10,9... | collective-permute-start | bytes 491528 | tf_op jit(solution)/shard_map/ppermute | solution.py:24
  110.0 20.6 %collective-permute-start.1 = (bf16[1,40,2048]{2,1,0:T(8,128)(2,1)}, bf16[1,40,2048]{2,1,0:T(8,128)(2,1)S(1)}, u32[]{:S(2)}, u32[]{:S(2)}) collective-permute-start(bf16[1,40,2048]{2,1,0:T(8,128)(2,1)} %get-tuple-element.19), channel_id=1, source_target_pairs={{0,14},{1,15},{2,0},{3,1},{4,2},{5,3},{6,4},{7,5},{8,6},{9,7},{10,... | collective-permute-start | bytes 491528 | tf_op jit(solution)/shard_map/ppermute | solution.py:24
  110.8 19.8 %collective-permute-start.2 = (bf16[1,40,2048]{2,1,0:T(8,128)(2,1)}, bf16[1,40,2048]{2,1,0:T(8,128)(2,1)S(1)}, u32[]{:S(2)}, u32[]{:S(2)}) collective-permute-start(bf16[1,40,2048]{2,1,0:T(8,128)(2,1)} %get-tuple-element.18), channel_id=1, source_target_pairs={{0,13},{1,14},{2,15},{3,0},{4,1},{5,2},{6,3},{7,4},{8,5},{9,6},{10... | collective-permute-start | bytes 491528 | tf_op jit(solution)/shard_map/ppermute | solution.py:24
  111.9 19.4 %collective-permute-start.3 = (bf16[1,40,2048]{2,1,0:T(8,128)(2,1)}, bf16[1,40,2048]{2,1,0:T(8,128)(2,1)S(1)}, u32[]{:S(2)}, u32[]{:S(2)}) collective-permute-start(bf16[1,40,2048]{2,1,0:T(8,128)(2,1)} %get-tuple-element.17), channel_id=1, source_target_pairs={{0,12},{1,13},{2,14},{3,15},{4,0},{5,1},{6,2},{7,3},{8,4},{9,5},{1... | collective-permute-start | bytes 491528 | tf_op jit(solution)/shard_map/ppermute | solution.py:24
  112.9 21.7 %collective-permute-start.4 = (bf16[1,40,2048]{2,1,0:T(8,128)(2,1)}, bf16[1,40,2048]{2,1,0:T(8,128)(2,1)S(1)}, u32[]{:S(2)}, u32[]{:S(2)}) collective-permute-start(bf16[1,40,2048]{2,1,0:T(8,128)(2,1)} %get-tuple-element.16), channel_id=1, source_target_pairs={{0,11},{1,12},{2,13},{3,14},{4,15},{5,0},{6,1},{7,2},{8,3},{9,4},{... | collective-permute-start | bytes 491528 | tf_op jit(solution)/shard_map/ppermute | solution.py:24
  116.0 23.7 %collective-permute-start.5 = (bf16[1,40,2048]{2,1,0:T(8,128)(2,1)}, bf16[1,40,2048]{2,1,0:T(8,128)(2,1)S(1)}, u32[]{:S(2)}, u32[]{:S(2)}) collective-permute-start(bf16[1,40,2048]{2,1,0:T(8,128)(2,1)} %get-tuple-element.15), channel_id=1, source_target_pairs={{0,10},{1,11},{2,12},{3,13},{4,14},{5,15},{6,0},{7,1},{8,2},{9,3},... | collective-permute-start | bytes 491528 | tf_op jit(solution)/shard_map/ppermute | solution.py:24
  130.6 13.0 %collective-permute-start.6 = (bf16[1,40,2048]{2,1,0:T(8,128)(2,1)}, bf16[1,40,2048]{2,1,0:T(8,128)(2,1)S(1)}, u32[]{:S(2)}, u32[]{:S(2)}) collective-permute-start(bf16[1,40,2048]{2,1,0:T(8,128)(2,1)} %get-tuple-element.14), channel_id=1, source_target_pairs={{0,9},{1,10},{2,11},{3,12},{4,13},{5,14},{6,15},{7,0},{8,1},{9,2},... | collective-permute-start | bytes 491528 | tf_op jit(solution)/shard_map/ppermute | solution.py:24
  130.6 13.5 %collective-permute-start.7 = (bf16[1,40,2048]{2,1,0:T(8,128)(2,1)}, bf16[1,40,2048]{2,1,0:T(8,128)(2,1)S(1)}, u32[]{:S(2)}, u32[]{:S(2)}) collective-permute-start(bf16[1,40,2048]{2,1,0:T(8,128)(2,1)} %get-tuple-element.13), channel_id=1, source_target_pairs={{0,8},{1,9},{2,10},{3,11},{4,12},{5,13},{6,14},{7,15},{8,0},{9,1},... | collective-permute-start | bytes 491528 | tf_op jit(solution)/shard_map/ppermute | solution.py:24
  131.3 15.7 %collective-permute-start.8 = (bf16[1,40,2048]{2,1,0:T(8,128)(2,1)}, bf16[1,40,2048]{2,1,0:T(8,128)(2,1)S(1)}, u32[]{:S(2)}, u32[]{:S(2)}) collective-permute-start(bf16[1,40,2048]{2,1,0:T(8,128)(2,1)} %get-tuple-element.12), channel_id=1, source_target_pairs={{0,7},{1,8},{2,9},{3,10},{4,11},{5,12},{6,13},{7,14},{8,15},{9,0},... | collective-permute-start | bytes 491528 | tf_op jit(solution)/shard_map/ppermute | solution.py:24
  134.6 20.7 %collective-permute-start.9 = (bf16[1,40,2048]{2,1,0:T(8,128)(2,1)}, bf16[1,40,2048]{2,1,0:T(8,128)(2,1)S(1)}, u32[]{:S(2)}, u32[]{:S(2)}) collective-permute-start(bf16[1,40,2048]{2,1,0:T(8,128)(2,1)} %get-tuple-element.11), channel_id=1, source_target_pairs={{0,6},{1,7},{2,8},{3,9},{4,10},{5,11},{6,12},{7,13},{8,14},{9,15},... | collective-permute-start | bytes 491528 | tf_op jit(solution)/shard_map/ppermute | solution.py:24
  139.7 18.5 %collective-permute-start.10 = (bf16[1,40,2048]{2,1,0:T(8,128)(2,1)}, bf16[1,40,2048]{2,1,0:T(8,128)(2,1)S(1)}, u32[]{:S(2)}, u32[]{:S(2)}) collective-permute-start(bf16[1,40,2048]{2,1,0:T(8,128)(2,1)} %get-tuple-element.10), channel_id=1, source_target_pairs={{0,5},{1,6},{2,7},{3,8},{4,9},{5,10},{6,11},{7,12},{8,13},{9,14},{... | collective-permute-start | bytes 491528 | tf_op jit(solution)/shard_map/ppermute | solution.py:24
  143.7 14.6 %collective-permute-start.11 = (bf16[1,40,2048]{2,1,0:T(8,128)(2,1)}, bf16[1,40,2048]{2,1,0:T(8,128)(2,1)S(1)}, u32[]{:S(2)}, u32[]{:S(2)}) collective-permute-start(bf16[1,40,2048]{2,1,0:T(8,128)(2,1)} %get-tuple-element.9), channel_id=1, source_target_pairs={{0,4},{1,5},{2,6},{3,7},{4,8},{5,9},{6,10},{7,11},{8,12},{9,13},{1... | collective-permute-start | bytes 491528 | tf_op jit(solution)/shard_map/ppermute | solution.py:24
  144.1 14.2 %collective-permute-start.12 = (bf16[1,40,2048]{2,1,0:T(8,128)(2,1)}, bf16[1,40,2048]{2,1,0:T(8,128)(2,1)S(1)}, u32[]{:S(2)}, u32[]{:S(2)}) collective-permute-start(bf16[1,40,2048]{2,1,0:T(8,128)(2,1)} %get-tuple-element.8), channel_id=1, source_target_pairs={{0,3},{1,4},{2,5},{3,6},{4,7},{5,8},{6,9},{7,10},{8,11},{9,12},{10... | collective-permute-start | bytes 491528 | tf_op jit(solution)/shard_map/ppermute | solution.py:24
  147.0 20.9 %collective-permute-start.13 = (bf16[1,40,2048]{2,1,0:T(8,128)(2,1)S(1)}, bf16[1,40,2048]{2,1,0:T(8,128)(2,1)S(1)}, u32[]{:S(2)}, u32[]{:S(2)}) collective-permute-start(bf16[1,40,2048]{2,1,0:T(8,128)(2,1)S(1)} %get-tuple-element.7), channel_id=1, source_target_pairs={{0,2},{1,3},{2,4},{3,5},{4,6},{5,7},{6,8},{7,9},{8,10},{9,11},{10,... | collective-permute-start | bytes 491528 | tf_op jit(solution)/shard_map/ppermute | solution.py:24
  155.3 12.6 %collective-permute-start.14 = (bf16[1,40,2048]{2,1,0:T(8,128)(2,1)S(1)}, bf16[1,40,2048]{2,1,0:T(8,128)(2,1)S(1)}, u32[]{:S(2)}, u32[]{:S(2)}) collective-permute-start(bf16[1,40,2048]{2,1,0:T(8,128)(2,1)S(1)} %get-tuple-element.6), channel_id=1, source_target_pairs={{0,1},{1,2},{2,3},{3,4},{4,5},{5,6},{6,7},{7,8},{8,9},{9,10},{10,1... | collective-permute-start | bytes 491528 | tf_op jit(solution)/shard_map/ppermute | solution.py:24
  184.5 4.7 %copy-start.13 = (f32[48,4,2]{0,2,1:T(2,128)S(1)}, f32[48,4,2]{0,2,1:T(2,128)}, u32[]{:S(2)}) copy-start(f32[48,4,2]{0,2,1:T(2,128)} %param.27) | copy-start | bytes 4612
  184.5 5.3 %copy-start.16 = (f32[48,4]{0,1:T(4,128)S(1)}, f32[48,4]{0,1:T(4,128)}, u32[]{:S(2)}) copy-start(f32[48,4]{0,1:T(4,128)} %param.26) | copy-start | bytes 2308
  184.5 65.3 %copy-start.6 = (pred[192,2,640]{2,0,1:T(32,128)(4,1)S(1)}, pred[192,2,640]{2,0,1:T(32,128)(4,1)}, u32[]{:S(2)}) copy-start(pred[192,2,640]{2,0,1:T(32,128)(4,1)} %get-tuple-element.27) | copy-start | bytes 737284
  184.5 65.3 %all-to-all-start.1 = ((bf16[16,40,2048]{2,1,0:T(8,128)(2,1)}), bf16[16,40,2048]{2,1,0:T(8,128)(2,1)}, u32[]{:S(2)}, u32[]{:S(2)}) async-start(bf16[16,40,2048]{2,1,0:T(8,128)(2,1)} %bitcast.69), calls=%async_computation.1 | async-start | bytes 5242880 | tf_op jit(solution)/shard_map/all_to_all | solution.py:182
  (8 other events, 12.1 us)
Sparse Core Ops, SparseCore 0:
  8.9 35.5 all-gather.2
  46.6 51.8 all-gather.4
